TPU v7x, 32 devices: a whole 2x2x4 slice. The times are simulated.
32 devices in a mesh: fs: 8 (over z, x), tp: 4 (over y, core).
Axes of the slice: x: 2, y: 2, z: 4, core: 2. Of those that a mesh axis runs over, the one named last changes fastest.
Arguments:
- tokens: bfloat16 [1536, 2048], P('fs'), may hold values from -6 to 6
- norm_gain: float32 [2048], P('fs'), may hold values from 0.1 to 1.9
- expert_gate: float32 [16, 2048, 1024], P(None, 'fs', 'tp'), may hold values from -0.125 to 0.125
- expert_up: float32 [16, 2048, 1024], P(None, 'fs', 'tp'), may hold values from -0.125 to 0.125
- expert_down: float32 [16, 1024, 2048], P(None, 'fs', 'tp'), may hold values from -0.1875 to 0.1875
- shared_gate: float32 [2048, 1024], P('fs', 'tp'), may hold values from -0.125 to 0.125
- shared_up: float32 [2048, 1024], P('fs', 'tp'), may hold values from -0.125 to 0.125
- shared_down: float32 [1024, 2048], P('fs', 'tp'), may hold values from -0.1875 to 0.1875
- expert_ids: int32 [1536, 8], P('fs'), may hold values from 0 to 15, all different within a row; in each aligned block of 192 rows (0 to 191, 192 to 383, ...) at most 192 rows name the same one
- route_weights: float32 [1536, 8], P('fs'), may hold values from 0.25 to 1
Outputs:
- gate_ready: bfloat16 [16, 2048, 1024], P('fs', None, 'tp')
- up_ready: bfloat16 [16, 2048, 1024], P('fs', None, 'tp')
- down_ready: bfloat16 [16, 1024, 2048], P('fs', None, 'tp')
- shared_gate_ready: bfloat16 [2048, 1024], P(None, 'tp')
- shared_up_ready: bfloat16 [2048, 1024], P(None, 'tp')
- shared_down_ready: bfloat16 [1024, 2048], P(None, 'tp')
- mixed: bfloat16 [1536, 2048], P('fs', 'tp')
Inputs may be any that keep to these rules, and one draw needn't show every extreme that they name: `expert_ids`: each row names 8 different experts. Among the 192 rows of one index of fs no expert is named more than 192 times, and in every draw some expert is named exactly 192 times there.
All inputs are finite; a program needn't handle non-finite values.
Results may differ from a plain program's by a relative error of at most 0.0085.
Values may be sent and summed in bfloat16 or wider, within the bound.
A program may use at most 128 MiB of HBM per device.

v0:
```python
import jax
import jax.numpy as jnp
from jax import lax
from jax.sharding import PartitionSpec as P

TOP_K = 8


EPS = 1e-06


def expert_hidden(rows, gate_new, up_new):
    first = jnp.einsum("secn,enf->secf", rows, gate_new, preferred_element_type=jnp.float32)
    second = jnp.einsum("secn,enf->secf", rows, up_new, preferred_element_type=jnp.float32)
    return (jax.nn.silu(first) * second).astype(jnp.bfloat16)


def body(
    tokens,
    norm_gain,
    expert_gate,
    expert_up,
    expert_down,
    shared_gate,
    shared_up,
    shared_down,
    expert_ids,
    route_weights,
):
    groups = lax.axis_size("fs")
    experts = expert_gate.shape[0]
    per_group = experts // groups
    tok_count = tokens.shape[0]
    capacity = 2 * tok_count * TOP_K // experts
    gate_local = (expert_gate * norm_gain[None, :, None]).astype(jnp.bfloat16)
    up_local = (expert_up * norm_gain[None, :, None]).astype(jnp.bfloat16)
    down_local = expert_down.astype(jnp.bfloat16)
    gate_local = gate_local.reshape((groups, per_group) + gate_local.shape[1:])
    up_local = up_local.reshape((groups, per_group) + up_local.shape[1:])
    down_local = down_local.reshape((groups, per_group) + down_local.shape[1:])
    shared_first_local = (shared_gate * norm_gain[:, None]).astype(jnp.bfloat16)
    shared_second_local = (shared_up * norm_gain[:, None]).astype(jnp.bfloat16)
    shared_third_local = shared_down.astype(jnp.bfloat16)
    gate_moved, up_moved, down_moved = (
        lax.all_to_all(gate_local, "fs", split_axis=0, concat_axis=2, tiled=True),
        lax.all_to_all(up_local, "fs", split_axis=0, concat_axis=2, tiled=True),
        lax.all_to_all(down_local, "fs", split_axis=0, concat_axis=2, tiled=True),
    )
    down_ready = down_moved[0]
    gate_ready = gate_moved[0]
    up_ready = up_moved[0]
    shared_gate_ready, shared_up_ready, shared_down_ready = (
        lax.all_gather(shared_first_local, "fs", axis=0, tiled=True),
        lax.all_gather(shared_second_local, "fs", axis=0, tiled=True),
        lax.all_gather(shared_third_local, "fs", axis=0, tiled=True),
    )
    wide = tokens.astype(jnp.float32)
    normed = (wide * lax.rsqrt(jnp.mean(wide * wide, axis=-1, keepdims=True) + EPS)).astype(
        jnp.bfloat16
    )
    chosen = expert_ids.reshape(-1)
    onehot = (chosen[:, None] == jnp.arange(experts, dtype=jnp.int32)[None, :]).astype(jnp.int32)
    ranks = jnp.sum(jnp.cumsum(onehot, axis=0) * onehot, axis=1) - 1
    owners = jnp.arange(tok_count * TOP_K, dtype=jnp.int32) // TOP_K
    slot_token = jnp.zeros((experts, capacity), jnp.int32).at[chosen, ranks].set(owners)
    outgoing = normed[slot_token.reshape(-1)].reshape(groups, per_group, capacity, normed.shape[1])
    share = capacity // lax.axis_size("tp")
    mine = lax.dynamic_slice_in_dim(outgoing, lax.axis_index("tp") * share, share, 2)
    arrived = lax.all_to_all(mine, "fs", split_axis=0, concat_axis=0, tiled=True)
    hidden = expert_hidden(lax.all_gather(arrived, "tp", axis=2, tiled=True), gate_ready, up_ready)
    shared_first = jnp.dot(normed, shared_gate_ready, preferred_element_type=jnp.float32)
    shared_second = jnp.dot(normed, shared_up_ready, preferred_element_type=jnp.float32)
    shared_hidden = (jax.nn.silu(shared_first) * shared_second).astype(jnp.bfloat16)[None, None]
    columns = down_ready.shape[2]
    routed_piece = lax.all_gather(hidden, "tp", axis=3, tiled=True)
    shared_piece = lax.all_gather(shared_hidden, "tp", axis=3, tiled=True)
    routed_total = jnp.einsum(
        "secf,efd->secd", routed_piece, down_ready, preferred_element_type=jnp.float32
    )
    shared_total = jnp.einsum(
        "abtf,fd->abtd", shared_piece, shared_down_ready, preferred_element_type=jnp.float32
    )
    returned = lax.all_to_all(
        routed_total.astype(jnp.bfloat16), "fs", split_axis=0, concat_axis=0, tiled=True
    )
    returned = returned.reshape(experts * capacity, columns)
    picked = (
        returned[chosen * capacity + ranks].astype(jnp.float32).reshape(tok_count, TOP_K, columns)
    )
    routed = jnp.sum(picked * route_weights[:, :, None], axis=1)
    mixed = (shared_total[0, 0] + routed).astype(jnp.bfloat16)
    return (
        gate_ready,
        up_ready,
        down_ready,
        shared_gate_ready,
        shared_up_ready,
        shared_down_ready,
        mixed,
    )


def solution(mesh):
    in_specs = (
        P("fs", None),
        P("fs"),
        P(None, "fs", "tp"),
        P(None, "fs", "tp"),
        P(None, "fs", "tp"),
        P("fs", "tp"),
        P("fs", "tp"),
        P("fs", "tp"),
        P("fs", None),
        P("fs", None),
    )
    out_specs = (
        P("fs", None, "tp"),
        P("fs", None, "tp"),
        P("fs", None, "tp"),
        P(None, "tp"),
        P(None, "tp"),
        P(None, "tp"),
        P("fs", "tp"),
    )
    return jax.shard_map(body, mesh=mesh, in_specs=in_specs, out_specs=out_specs, check_vma=False)
```

profile of v0, /device:TPU:30, one launch (start us, length us, event | category | flops | bytes accessed | tf_op | source)
XLA Modules:
  0.0 492.7 jit_solution(2639579314955655881)
XLA Ops:
  8.4 4.5 reduce-window.6
  15.3 6.2 %scatter_custom_fusion = s32[3072]{0:T(1024)S(1)} fusion(s32[1536]{0:T(1024)S(1)} %get-tuple-element.17, s32[1536]{0:T(1024)S(1)} %get-tuple-element.16, s32[]{:T(128)} %constant.45.clone.1), kind=kCustom, calls=%fused_computation.50 | custom fusion | bytes 12292
  21.5 1.4 fusion.5
  22.9 1.3 fusion.6
  24.2 15.9 %gather_fusion = bf16[3072,2048]{1,0:T(8,128)(2,1)} fusion(bf16[192,2048]{1,0:T(8,128)(2,1)S(1)} %fusion.6, s32[3072]{0:T(1024)S(1)} %broadcast_clamp_fusion), kind=kCustom, calls=%fused_computation | custom fusion | bytes 25178112 | tf_op jit(solution)/shard_map/gather | solution.py:66
  40.1 2.3 constant_dynamic-slice_fusion
  42.4 74.1 %all_to_all.55 = bf16[8,2,48,2048]{3,2,1,0:T(8,128)(2,1)S(1)} all-to-all(bf16[8,2,48,2048]{3,2,1,0:T(8,128)(2,1)S(1)} %constant_dynamic-slice_fusion), channel_id=1, replica_groups=mesh['fs'=8,'tp'=4] {'fs'}, dimensions={0} | all-to-all | bytes 6291456 | tf_op jit(solution)/shard_map/all_to_all | solution.py:69
  116.5 2.1 copy.36
  119.3 5.8 %multiply_convert_fusion = (bf16[16,256,256]{2,1,0:T(8,128)(2,1)S(1)}, bf16[16,256,256]{2,1,0:T(8,128)(2,1)}) fusion(f32[16,256,256]{2,1,0:T(8,128)} %param.13, f32[256]{0:T(256)S(1)} %copy-done.8, f32[16,256,256]{2,1,0:T(8,128)} %param.12), kind=kLoop, calls=%fused_computation.3 | loop fusion | flops 4194304 | bytes 12583936 | tf_op jit(solution)/shard_map/convert_element_type | solution.py:36
  125.1 51.4 %all_to_all.56 = bf16[8,2,256,256]{3,2,1,0:T(8,128)(2,1)} all-to-all(bf16[8,2,256,256]{3,2,1,0:T(8,128)(2,1)S(1)} %bitcast.80), channel_id=1, replica_groups=mesh['fs'=8,'tp'=4] {'fs'}, dimensions={0} | all-to-all | bytes 4194304 | tf_op jit(solution)/shard_map/all_to_all | solution.py:46
  176.5 6.0 %all-to-all-start = ((bf16[8,2,256,256]{3,2,1,0:T(8,128)(2,1)}), bf16[8,2,256,256]{3,2,1,0:T(8,128)(2,1)S(1)}, u32[]{:S(2)}, u32[]{:S(2)}) async-start(bf16[8,2,256,256]{3,2,1,0:T(8,128)(2,1)} %bitcast), calls=%async_computation | async-start | bytes 4194304 | tf_op jit(solution)/shard_map/all_to_all | solution.py:45
  182.5 3.2 copy.31
  185.7 42.2 %all-to-all-done = bf16[8,2,256,256]{3,2,1,0:T(8,128)(2,1)S(1)} async-done(((bf16[8,2,256,256]{3,2,1,0:T(8,128)(2,1)}), bf16[8,2,256,256]{3,2,1,0:T(8,128)(2,1)S(1)}, u32[]{:S(2)}, u32[]{:S(2)}) %all-to-all-start) | async-done | bytes 2097184 | tf_op jit(solution)/shard_map/all_to_all | solution.py:45
  227.9 1.5 copy.30
  229.4 10.4 %fusion.19 = f32[2,256,8,192]{1,3,2,0:T(8,128)} fusion(bf16[2,2048,256,1]{2,1,3,0:T(8,128)(2,1)} %bitcast.84, bf16[8,2,192,2048]{3,2,0,1:T(8,128)(2,1)} %all-gather.13.cloned.1.call-done), kind=kOutput, calls=%fused_computation.58 | convolution fusion | flops 3221225472 | bytes 17825792 | tf_op jit(solution)/shard_map/secn,enf->secf/dot_general | solution.py:14
  239.8 10.5 %fusion.1 = bf16[8,2,192,256]{3,2,0,1:T(8,128)(2,1)} fusion(f32[2,256,8,192]{1,3,2,0:T(8,128)} %fusion.19, bf16[2,2048,256,1]{2,1,3,0:T(8,128)(2,1)S(1)} %bitcast.87, bf16[8,2,192,2048]{3,2,0,1:T(8,128)(2,1)} %all-gather.13.cloned.1.call-done), kind=kOutput, calls=%fused_computation.8 | convolution fusion | flops 3225944064 | bytes 19398656 | tf_op jit(solution)/shard_map/secn,enf->secf/dot_general | solution.py:13
  250.3 3.8 convert_element_type.53
  254.2 6.1 %all-to-all-start.2 = ((bf16[8,2,128,512]{3,2,1,0:T(8,128)(2,1)}), bf16[8,2,128,512]{3,2,1,0:T(8,128)(2,1)S(1)}, u32[]{:S(2)}, u32[]{:S(2)}) async-start(bf16[8,2,128,512]{3,2,1,0:T(8,128)(2,1)} %bitcast.8), calls=%async_computation.2 | async-start | bytes 4194304 | tf_op jit(solution)/shard_map/all_to_all | solution.py:47
  261.1 45.2 %all-to-all-done.2 = bf16[8,2,128,512]{3,2,1,0:T(8,128)(2,1)S(1)} async-done(((bf16[8,2,128,512]{3,2,1,0:T(8,128)(2,1)}), bf16[8,2,128,512]{3,2,1,0:T(8,128)(2,1)S(1)}, u32[]{:S(2)}, u32[]{:S(2)}) %all-to-all-start.2) | async-done | bytes 2097184 | tf_op jit(solution)/shard_map/all_to_all | solution.py:47
  306.3 1.5 copy.32
  307.9 7.0 %convert_bitcast_fusion = bf16[8,2,192,512]{3,2,0,1:T(8,128)(2,1)S(1)} fusion(bf16[8,2,192,1024]{3,2,0,1:T(8,128)(2,1)} %all-gather.15.cloned.1.call-done, bf16[2,1024,512,1]{2,1,3,0:T(8,128)(2,1)} %bitcast.88), kind=kOutput, calls=%fused_computation.14 | convolution fusion | flops 3222798336 | bytes 11534336 | tf_op jit(solution)/shard_map/secf,efd->secd/dot_general | solution.py:77
  314.9 1.9 copy.37
  316.8 6.7 %all-to-all-start.4 = ((bf16[8,2,192,512]{3,2,1,0:T(8,128)(2,1)}), bf16[8,2,192,512]{3,2,1,0:T(8,128)(2,1)}, u32[]{:S(2)}, u32[]{:S(2)}) async-start(bf16[8,2,192,512]{3,2,1,0:T(8,128)(2,1)} %copy.37), calls=%async_computation.4 | async-start | bytes 6291456 | tf_op jit(solution)/shard_map/all_to_all | solution.py:83
  325.2 44.1 %all-gather.7.cloned.1.call-done = bf16[2048,256]{1,0:T(8,128)(2,1)} async-done(((bf16[256,256]{1,0:T(8,128)(2,1)}), bf16[2048,256]{1,0:T(8,128)(2,1)}) %all-gather.7.cloned.1.call-update) | async-done | bytes 1048592 | tf_op jit(solution)/shard_map/all_gather | solution.py:53
  369.3 53.6 %all-gather.9.cloned.1.call-done = bf16[2048,256]{1,0:T(8,128)(2,1)} async-done(((bf16[256,256]{1,0:T(8,128)(2,1)}), bf16[2048,256]{1,0:T(8,128)(2,1)}) %all-gather.9.cloned.1.call-update) | async-done | bytes 1048592 | tf_op jit(solution)/shard_map/all_gather | solution.py:54
  423.0 41.6 %all-gather.11.cloned.1.call-done = bf16[1024,512]{1,0:T(8,128)(2,1)} async-done(((bf16[128,512]{1,0:T(8,128)(2,1)}), bf16[1024,512]{1,0:T(8,128)(2,1)}) %all-gather.11.cloned.1.call-update) | async-done | bytes 1048592 | tf_op jit(solution)/shard_map/all_gather | solution.py:55
  464.5 1.6 fusion.18
  466.1 1.6 fusion.8
  467.7 6.1 %all-gather = bf16[192,1024]{1,0:T(8,128)(2,1)S(1)} all-gather(bf16[192,256]{1,0:T(8,128)(2,1)S(1)} %fusion.8), channel_id=2, replica_groups=mesh['fs'=8,'tp'=4] {'tp'}, dimensions={1}, use_global_device_ids=true | all-gather | bytes 491520 | tf_op jit(solution)/shard_map/all_gather | solution.py:76
  473.9 7.2 %gather_fusion.1 = bf16[1536,512]{1,0:T(8,128)(2,1)S(1)} fusion(bf16[3072,512]{1,0:T(8,128)(2,1)} %bitcast.25, s32[2048]{0:T(1024)S(1)} %pad_clamp_fusion), kind=kCustom, calls=%fused_computation.1 | custom fusion | bytes 3151872 | tf_op jit(solution)/shard_map/gather | solution.py:88
  481.2 1.0 fusion
  482.2 1.1 fusion.7
  (55 shorter events, 9.6 us)
Async XLA Ops:
  7.2 222.2 %all-gather.13.cloned.1.call-start = ((), (), s32[]{:S(2)}) async-start(), calls=%async_computation.8 | async-start | bytes 15728640 | tf_op jit(solution)/shard_map/all_gather | solution.py:70
  118.6 0.7 copy-start.8
  176.5 51.5 %all-to-all-start = ((bf16[8,2,256,256]{3,2,1,0:T(8,128)(2,1)}), bf16[8,2,256,256]{3,2,1,0:T(8,128)(2,1)S(1)}, u32[]{:S(2)}, u32[]{:S(2)}) async-start(bf16[8,2,256,256]{3,2,1,0:T(8,128)(2,1)} %bitcast), calls=%async_computation | async-start | bytes 4194304 | tf_op jit(solution)/shard_map/all_to_all | solution.py:45
  182.5 125.4 %all-gather.15.cloned.1.call-start = ((), (), s32[]{:S(2)}) async-start(), calls=%async_computation.9 | async-start | bytes 7864320 | tf_op jit(solution)/shard_map/all_gather | solution.py:75
  229.4 10.4 %copy-start.2 = (bf16[1,2,8,256,256]{4,3,2,1,0:T(8,128)(2,1)S(1)}, bf16[1,2,8,256,256]{4,3,2,1,0:T(8,128)(2,1)}, u32[]{:S(2)}) copy-start(bf16[1,2,8,256,256]{4,3,2,1,0:T(8,128)(2,1)} %copy.30) | copy-start | bytes 6291460
  254.1 6.1 %copy-start.5 = (f32[256,256]{1,0:T(8,128)S(1)}, f32[256,256]{1,0:T(8,128)}, u32[]{:S(2)}) copy-start(f32[256,256]{1,0:T(8,128)} %param.16) | copy-start | bytes 786436
  254.2 6.1 %copy-start.6 = (f32[256,256]{1,0:T(8,128)S(1)}, f32[256,256]{1,0:T(8,128)}, u32[]{:S(2)}) copy-start(f32[256,256]{1,0:T(8,128)} %param.15) | copy-start | bytes 786436
  254.2 52.2 %all-to-all-start.2 = ((bf16[8,2,128,512]{3,2,1,0:T(8,128)(2,1)}), bf16[8,2,128,512]{3,2,1,0:T(8,128)(2,1)S(1)}, u32[]{:S(2)}, u32[]{:S(2)}) async-start(bf16[8,2,128,512]{3,2,1,0:T(8,128)(2,1)} %bitcast.8), calls=%async_computation.2 | async-start | bytes 4194304 | tf_op jit(solution)/shard_map/all_to_all | solution.py:47
  260.3 109.0 %all-gather.7.cloned.1.call-start = ((), (), s32[]{:S(2)}) async-start(), calls=%async_computation.5 | async-start | bytes 1179648 | tf_op jit(solution)/shard_map/all_gather | solution.py:53
  316.8 7.6 %copy-start.4 = (f32[128,512]{1,0:T(8,128)S(1)}, f32[128,512]{1,0:T(8,128)}, u32[]{:S(2)}) copy-start(f32[128,512]{1,0:T(8,128)} %param.17) | copy-start | bytes 786436
  316.8 8.3 %copy-start.7 = (f32[192,8]{0,1:T(8,128)S(1)}, f32[192,8]{0,1:T(8,128)}, u32[]{:S(2)}) copy-start(f32[192,8]{0,1:T(8,128)} %param.19) | copy-start | bytes 18436
  316.8 157.1 %all-to-all-start.4 = ((bf16[8,2,192,512]{3,2,1,0:T(8,128)(2,1)}), bf16[8,2,192,512]{3,2,1,0:T(8,128)(2,1)}, u32[]{:S(2)}, u32[]{:S(2)}) async-start(bf16[8,2,192,512]{3,2,1,0:T(8,128)(2,1)} %copy.37), calls=%async_computation.4 | async-start | bytes 6291456 | tf_op jit(solution)/shard_map/all_to_all | solution.py:83
  323.5 99.5 %all-gather.9.cloned.1.call-start = ((), (), s32[]{:S(2)}) async-start(), calls=%async_computation.6 | async-start | bytes 1179648 | tf_op jit(solution)/shard_map/all_gather | solution.py:54
  324.1 140.5 %all-gather.11.cloned.1.call-start = ((), (), s32[]{:S(2)}) async-start(), calls=%async_computation.7 | async-start | bytes 1179648 | tf_op jit(solution)/shard_map/all_gather | solution.py:55
  473.9 8.3 %copy-start.1 = (bf16[1024,512]{1,0:T(8,128)(2,1)S(1)}, bf16[1024,512]{1,0:T(8,128)(2,1)}, u32[]{:S(2)}) copy-start(bf16[1024,512]{1,0:T(8,128)(2,1)} %all-gather.11.cloned.1.call-done) | copy-start | bytes 3145732
  481.1 2.1 copy-start
  481.1 3.0 copy-start.3
Sparse Core Ops, SparseCore 0:
  118.7 82.0 all-gather.12
  250.5 47.1 all-gather.14
  300.4 68.8 all-gather.6
  371.9 51.0 all-gather.8
  425.5 38.9 all-gather.10
where the time goes:
time: 498 us; the launch traced here: 493 us
  waiting for transfers between devices  227 us (46%)
  blocking collectives  132 us (27%)
  local copies, waits for them, and re-layouts  47 us (9%)
  matrix products  32.2 us (6%)
  other arithmetic  21.2 us (4%)
  starting transfers between devices  19.2 us (4%)
  between operations  14 us (3%)
    all_to_all x1, blocking collectives, body(): lax.all_to_all(mine, 'fs', split_axis=0, concat_axis=0, tiled=True)  74.1 us
    all_gather x1, waiting for transfers between devices, body(): lax.all_gather(shared_second_local, 'fs', axis=0, tiled=True)  53.6 us
    all_to_all x1, blocking collectives, body(): lax.all_to_all(up_local, 'fs', split_axis=0, concat_axis=2, tiled=True)  51.4 us
    all_to_all x1, waiting for transfers between devices, body(): lax.all_to_all(down_local, 'fs', split_axis=0, concat_axis=2, tiled=True)  45.2 us
    all_gather x1, waiting for transfers between devices, body(): lax.all_gather(shared_first_local, 'fs', axis=0, tiled=True)  44.1 us
    all_to_all x1, waiting for transfers between devices, body(): lax.all_to_all(gate_local, 'fs', split_axis=0, concat_axis=2, tiled=True)  42.2 us
    all_gather x1, waiting for transfers between devices, body(): lax.all_gather(shared_third_local, 'fs', axis=0, tiled=True)  41.6 us
    gather x1, local copies, waits for them, and re-layouts, body(): normed[slot_token.reshape(-1)]  15.9 us
  transfers between devices with their start and end apart: 8, of which 5 were waited for; matrix products, arithmetic and copies ran while one was open for 6% of the time, Pallas kernels for 0%

commit v1 on v0

--- a/solution.py
+++ b/solution.py
@@ -1,12 +1,589 @@
+import functools
 import jax
 import jax.numpy as jnp
 from jax import lax
+from jax.experimental import pallas as pl
+from jax.experimental.pallas import tpu as pltpu
 from jax.sharding import PartitionSpec as P
 
 TOP_K = 8
 
 
 EPS = 1e-06
+
+MESH = pl.DeviceIdType.MESH
+LANES = 128
+
+
+def flip(value, mask, extent):
+    result, bit = 0, 1
+    while bit < extent:
+        digit = (value // bit) % 2
+        result = result + bit * ((1 - digit) if mask & bit else digit)
+        bit *= 2
+    return result
+
+
+def fused_kernel(
+    groups,
+    ranks,
+    ext,
+    gain,
+    eg,
+    eu,
+    ed,
+    sg,
+    su,
+    sd,
+    out_g,
+    out_u,
+    out_d,
+    out_sg,
+    out_su,
+    out_sd,
+    out_mixed,
+    st_g,
+    st_u,
+    st_d,
+    sb_g,
+    sb_u,
+    sb_d,
+    rv_g,
+    rv_u,
+    rv_d,
+    sh,
+    tok,
+    hid,
+    shid,
+    res_s,
+    res_r,
+    own_out,
+    load_sem,
+    loc_sem,
+    a2a_send,
+    a2a_recv,
+    tok_send,
+    tok_recv,
+    tok_csend,
+    tok_crecv,
+    sh_send,
+    sh_recv,
+    hid_csend,
+    hid_ysend,
+    hid_fsend,
+    hid_recv,
+    shid_send,
+    shid_recv,
+    res_send,
+    res_recv,
+    out_sem,
+    shout_sem,
+):
+    nx = 2
+    nz = groups // nx
+    me = lax.axis_index("fs")
+    tp = lax.axis_index("tp")
+    z, x = me // nx, me % nx
+    core = tp % 2
+    partner = flip(tp, 1, ranks)
+    across = flip(tp, 2, ranks)
+    per = eg.shape[0] // groups
+    experts = eg.shape[0]
+    rows_w = eg.shape[1]
+    rows_d = ed.shape[1]
+    tok_count = ext.shape[0]
+    width = st_d.shape[2] * ranks
+    half = tok_count // 2
+    hcols = eg.shape[2]
+    dcols = ed.shape[2]
+    hw = dcols // 2
+
+    loads = [
+        pltpu.make_async_copy(a, b, load_sem.at[i])
+        for i, (a, b) in enumerate(((eg, st_g), (eu, st_u), (ed, st_d)))
+    ]
+    for load in loads:
+        load.start()
+    own_tok = pltpu.make_async_copy(ext, tok.at[me], loc_sem.at[3])
+    own_tok.start()
+
+    barrier = pltpu.get_barrier_semaphore()
+    for o in range(1, groups):
+        pl.semaphore_signal(
+            barrier, inc=1, device_id={"fs": flip(me, o, groups)}, device_id_type=MESH
+        )
+    for o in range(1, ranks):
+        pl.semaphore_signal(
+            barrier, inc=1, device_id={"tp": flip(tp, o, ranks)}, device_id_type=MESH
+        )
+    pl.semaphore_wait(barrier, groups + ranks - 2)
+
+    mine = pl.ds(core * half, half)
+    theirs = pl.ds((1 - core) * half, half)
+
+    def fs_copy(src, dst, send, recv, target):
+        return pltpu.make_async_remote_copy(
+            src_ref=src,
+            dst_ref=dst,
+            send_sem=send,
+            recv_sem=recv,
+            device_id={"fs": target},
+            device_id_type=MESH,
+        )
+
+    def tp_copy(src, dst, send, recv, target):
+        return pltpu.make_async_remote_copy(
+            src_ref=src,
+            dst_ref=dst,
+            send_sem=send,
+            recv_sem=recv,
+            device_id={"tp": target},
+            device_id_type=MESH,
+        )
+
+    def tok_copy(block, slot, target, own=False):
+        src = ext.at[mine] if own else tok.at[block, mine]
+        return fs_copy(src, tok.at[block, mine], tok_send.at[slot], tok_recv.at[block], target)
+
+    def sh_copy(block, slot, target, own=False):
+        return fs_copy(sh.at[block], sh.at[block], sh_send.at[slot], sh_recv.at[block], target)
+
+    def gather_moves(copy, recv_copy, step, act):
+        other = 1 - x
+        if step == 0:
+
+            @pl.when(z + 1 < nz)
+            def _():
+                act(copy(me, 0, me + nx, True))
+
+            @pl.when(z >= 1)
+            def _():
+                act(copy(me, 1, me - nx, True))
+
+            act(copy(me, 2, z * nx + other, True))
+            return
+
+        @pl.when(z >= step)
+        def _():
+            block = me - step * nx
+            recv_copy(block)
+
+            @pl.when(z + 1 < nz)
+            def _():
+                act(copy(block, 4 * step - 1, me + nx))
+
+            act(copy(block, 4 * step, z * nx + other))
+
+        @pl.when(z + step < nz)
+        def _():
+            block = me + step * nx
+            recv_copy(block)
+
+            @pl.when(z >= 1)
+            def _():
+                act(copy(block, 4 * step + 1, me - nx))
+
+            act(copy(block, 4 * step + 2, z * nx + other))
+
+    def start(c):
+        c.start()
+
+    def wait_send(c):
+        c.wait_send()
+
+    def nothing(block):
+        pass
+
+    def tok_arrive(block):
+        tok_copy(block, 0, me).wait_recv()
+        core_copy(block).start()
+
+    def core_copy(block):
+        return tp_copy(
+            tok.at[block, mine],
+            tok.at[block, mine],
+            tok_csend.at[block],
+            tok_crecv.at[block],
+            partner,
+        )
+
+    def sh_arrive(block):
+        sh_copy(block, 0, me).wait_recv()
+
+    gather_moves(tok_copy, nothing, 0, start)
+
+    column = gain[...]
+    sh[me, 0] = (sg[...] * column).astype(jnp.bfloat16)
+    sh[me, 1] = (su[...] * column).astype(jnp.bfloat16)
+    sh[me, 2, 0:rows_d] = sd[:, 0:hw].astype(jnp.bfloat16)
+    sh[me, 2, rows_d : 2 * rows_d] = sd[:, hw:dcols].astype(jnp.bfloat16)
+
+    def cast(stage, sendbuf, scaled):
+        @pl.loop(0, experts)
+        def _(e):
+            value = stage[e]
+            if scaled:
+                value = value * gain[...]
+            sendbuf[e] = value.astype(jnp.bfloat16)
+
+    order = [o for o in (6, 4, 2, 7, 5, 3, 1) if o < groups]
+    order = order + [o for o in range(1, groups) if o not in order]
+
+    def a2a_copy(index, o):
+        sendbuf, recvbuf, rows = (
+            (sb_g, rv_g, rows_w),
+            (sb_u, rv_u, rows_w),
+            (sb_d, rv_d, rows_d),
+        )[index]
+        target = flip(me, o, groups)
+        return fs_copy(
+            sendbuf.at[pl.ds(target * per, per)],
+            recvbuf.at[:, pl.ds(me * rows, rows), :],
+            a2a_send.at[index, o],
+            a2a_recv.at[index, o],
+            target,
+        )
+
+    def a2a_own(index):
+        sendbuf, recvbuf, rows = (
+            (sb_g, rv_g, rows_w),
+            (sb_u, rv_u, rows_w),
+            (sb_d, rv_d, rows_d),
+        )[index]
+        return pltpu.make_async_copy(
+            sendbuf.at[pl.ds(me * per, per)],
+            recvbuf.at[:, pl.ds(me * rows, rows), :],
+            loc_sem.at[index],
+        )
+
+    def a2a_start(index):
+        for o in order:
+            a2a_copy(index, o).start()
+        a2a_own(index).start()
+
+    def a2a_arrive(index, recvbuf, out):
+        for o in order:
+            a2a_copy(index, o).wait_recv()
+        a2a_own(index).wait()
+        pltpu.make_async_copy(recvbuf, out, out_sem.at[index]).start()
+
+    loads[0].wait()
+    cast(st_g, sb_g, True)
+    gather_moves(sh_copy, nothing, 0, start)
+    gather_moves(tok_copy, tok_arrive, 1, start)
+    a2a_start(0)
+    loads[1].wait()
+    cast(st_u, sb_u, True)
+    gather_moves(sh_copy, sh_arrive, 1, start)
+    for step in range(2, nz):
+        gather_moves(tok_copy, tok_arrive, step, start)
+        if step == 2:
+            a2a_start(1)
+            loads[2].wait()
+            cast(st_d, sb_d, False)
+        gather_moves(sh_copy, sh_arrive, step, start)
+    a2a_start(2)
+
+    for zz in range(nz):
+        tok_arrive(zz * nx + (1 - x))
+    for zz in range(nz):
+        sh_arrive(zz * nx + (1 - x))
+    own_tok.wait()
+
+    def sh_out(block, part):
+        src_dst = (
+            (sh.at[block, 0], out_sg.at[pl.ds(block * rows_w, rows_w), :]),
+            (sh.at[block, 1], out_su.at[pl.ds(block * rows_w, rows_w), :]),
+            (sh.at[block, 2, pl.ds(0, rows_d)], out_sd.at[pl.ds(block * rows_d, rows_d), pl.ds(0, hw)]),
+            (sh.at[block, 2, pl.ds(rows_d, rows_d)], out_sd.at[pl.ds(block * rows_d, rows_d), pl.ds(hw, hw)]),
+        )[part]
+        return pltpu.make_async_copy(*src_dst, shout_sem.at[block, part])
+
+    for block in range(groups):
+        for part in range(4):
+            sh_out(block, part).start()
+
+    features = groups * rows_w
+
+    def shared_half(part):
+        total = jnp.zeros((tok_count, hcols), jnp.float32)
+        for block in range(groups):
+            total = total + jnp.dot(
+                ext[:, block * rows_w : (block + 1) * rows_w],
+                sh[block, part],
+                preferred_element_type=jnp.float32,
+            )
+        return total
+
+    shared_first = shared_half(0)
+    shared_second = shared_half(1)
+    shid[tp] = (jax.nn.silu(shared_first) * shared_second).astype(jnp.bfloat16)
+
+    def shid_copy(o):
+        return tp_copy(
+            shid.at[tp], shid.at[tp], shid_send.at[o], shid_recv.at[o], flip(tp, o, ranks)
+        )
+
+    def core_arrive(block):
+        tp_copy(
+            tok.at[block, theirs],
+            tok.at[block, theirs],
+            tok_csend.at[block],
+            tok_crecv.at[block],
+            partner,
+        ).wait_recv()
+
+    for o in range(1, groups):
+        core_arrive(flip(me, o, groups))
+
+    for o in range(1, ranks):
+        shid_copy(o).start()
+
+    a2a_arrive(0, rv_g, out_g)
+    a2a_arrive(1, rv_u, out_u)
+
+    def hid_core(block):
+        return tp_copy(
+            hid.at[tp, block], hid.at[tp, block], hid_csend.at[block], hid_recv.at[1, block], partner
+        )
+
+    def hid_across(block):
+        return tp_copy(
+            hid.at[tp, block], hid.at[tp, block], hid_ysend.at[block], hid_recv.at[2, block], across
+        )
+
+    def hid_forward(block):
+        return tp_copy(
+            hid.at[across, block],
+            hid.at[across, block],
+            hid_fsend.at[block],
+            hid_recv.at[3, block],
+            partner,
+        )
+
+    def turn(o):
+        return (me + o) % groups
+
+    @pl.loop(0, groups)
+    def _(o):
+        block = turn(o + 1)
+        rows = tok[block, :, 0:features]
+        for e in range(per):
+            first = jnp.dot(rows, rv_g[e], preferred_element_type=jnp.float32)
+            second = jnp.dot(rows, rv_u[e], preferred_element_type=jnp.float32)
+            hid[tp, block, e] = (jax.nn.silu(first) * second).astype(jnp.bfloat16)
+
+        @pl.when(o >= 1)
+        def _():
+            before = turn(o)
+            hid_across(before).start()
+            hid_core(before).start()
+
+    for o in range(1, ranks):
+        shid_copy(o).wait_recv()
+    hid_across(me).start()
+    hid_core(me).start()
+    for part in range(2):
+        total = jnp.zeros((tok_count, hw), jnp.float32)
+        for block in range(groups):
+            at = block * rows_d
+            total = total + jnp.dot(
+                shid[at // hcols, :, at % hcols : at % hcols + rows_d],
+                sh[block, 2, part * rows_d : (part + 1) * rows_d],
+                preferred_element_type=jnp.float32,
+            )
+        own_out[:, part * hw : (part + 1) * hw] = total
+
+    @pl.loop(0, groups)
+    def _(o):
+        block = turn(o + 1)
+        hid_across(block).wait_recv()
+        hid_forward(block).start()
+
+    a2a_arrive(2, rv_d, out_d)
+
+    lanes = lax.broadcasted_iota(jnp.int32, (tok_count, LANES), 1)
+
+    def res_copy(o):
+        target = turn(o)
+        return fs_copy(
+            res_s.at[target], res_r.at[me], res_send.at[o], res_recv.at[o], target
+        )
+
+    def block_out(block):
+        table = tok[block, :, features : features + LANES].astype(jnp.float32)
+        total = jnp.zeros((tok_count, dcols), jnp.float32)
+        for e in range(per):
+            expert = me * per + e
+            weight = jnp.sum(
+                jnp.where(
+                    (lanes == expert) | (lanes == expert + experts) | (lanes == expert + 2 * experts),
+                    table,
+                    0.0,
+                ),
+                axis=1,
+                keepdims=True,
+            )
+            out = jnp.zeros((tok_count, dcols), jnp.float32)
+            for r in range(ranks):
+                out = out + jnp.dot(
+                    hid[r, block, e],
+                    rv_d[e, r * hcols : (r + 1) * hcols],
+                    preferred_element_type=jnp.float32,
+                )
+            total = total + weight * out
+        return total
+
+    @pl.loop(1, groups + 1)
+    def _(o):
+        block = turn(o)
+        hid_core(block).wait_recv()
+        hid_forward(block).wait_recv()
+
+        @pl.when(o < groups)
+        def _():
+            res_s[block] = block_out(block).astype(jnp.bfloat16)
+
+        @pl.when(o == groups)
+        def _():
+            own_out[...] = own_out[...] + block_out(block)
+
+        @pl.when(o >= 2)
+        def _():
+            res_copy(o - 1).start()
+
+    for o in range(1, groups):
+        res_copy(o).wait_recv()
+        own_out[...] = own_out[...] + res_r[(me + groups - o) % groups].astype(jnp.float32)
+    out_mixed[...] = own_out[...].astype(jnp.bfloat16)
+
+    for o in range(1, groups):
+        res_copy(o).wait_send()
+    for index in range(3):
+        for o in order:
+            a2a_copy(index, o).wait_send()
+    for step in range(nz):
+        gather_moves(tok_copy, nothing, step, wait_send)
+        gather_moves(sh_copy, nothing, step, wait_send)
+    for o in range(1, groups):
+        core_copy(flip(me, o, groups)).wait_send()
+    for o in range(1, ranks):
+        shid_copy(o).wait_send()
+
+    @pl.loop(0, groups)
+    def _(o):
+        hid_core(o).wait_send()
+        hid_across(o).wait_send()
+        hid_forward(o).wait_send()
+
+    for index, (recvbuf, out) in enumerate(((rv_g, out_g), (rv_u, out_u), (rv_d, out_d))):
+        pltpu.make_async_copy(recvbuf, out, out_sem.at[index]).wait()
+    for block in range(groups):
+        for part in range(4):
+            sh_out(block, part).wait()
+
+
+def dense_body(
+    tokens,
+    norm_gain,
+    expert_gate,
+    expert_up,
+    expert_down,
+    shared_gate,
+    shared_up,
+    shared_down,
+    expert_ids,
+    route_weights,
+):
+    groups, ranks = lax.axis_size("fs"), lax.axis_size("tp")
+    experts, rows_w, hcols = expert_gate.shape
+    rows_d, dcols = expert_down.shape[1:]
+    per = experts // groups
+    tok_count, features = tokens.shape
+    wide = tokens.astype(jnp.float32)
+    normed = (wide * lax.rsqrt(jnp.mean(wide * wide, axis=-1, keepdims=True) + EPS)).astype(
+        jnp.bfloat16
+    )
+    named = expert_ids[:, :, None] == jnp.arange(experts, dtype=jnp.int32)[None, None, :]
+    table = jnp.sum(jnp.where(named, route_weights[:, :, None], 0.0), axis=1)
+    high = lax.reduce_precision(table, 8, 7)
+    middle = lax.reduce_precision(table - high, 8, 7)
+    low = table - high - middle
+    pad = jnp.zeros((tok_count, LANES - 3 * experts), jnp.bfloat16)
+    ext = jnp.concatenate(
+        [normed] + [v.astype(jnp.bfloat16) for v in (high, middle, low)] + [pad], axis=1
+    )
+    total = features + LANES
+    bf, f32 = jnp.bfloat16, jnp.float32
+    dma = pltpu.SemaphoreType.DMA
+    nz = groups // 2
+    any_space = pl.BlockSpec(memory_space=pl.ANY)
+    vmem = pl.BlockSpec(memory_space=pltpu.VMEM)
+    hidden = hcols * ranks
+    return pl.pallas_call(
+        functools.partial(fused_kernel, groups, ranks),
+        out_shape=(
+            jax.ShapeDtypeStruct((per, features, hcols), bf),
+            jax.ShapeDtypeStruct((per, features, hcols), bf),
+            jax.ShapeDtypeStruct((per, hidden, dcols), bf),
+            jax.ShapeDtypeStruct((features, hcols), bf),
+            jax.ShapeDtypeStruct((features, hcols), bf),
+            jax.ShapeDtypeStruct((hidden, dcols), bf),
+            jax.ShapeDtypeStruct((tok_count, dcols), bf),
+        ),
+        in_specs=[vmem, vmem, any_space, any_space, any_space, vmem, vmem, vmem],
+        out_specs=(any_space,) * 6 + (vmem,),
+        scratch_shapes=[
+            pltpu.VMEM((experts, rows_w, hcols), f32),
+            pltpu.VMEM((experts, rows_w, hcols), f32),
+            pltpu.VMEM((experts, rows_d, dcols), f32),
+            pltpu.VMEM((experts, rows_w, hcols), bf),
+            pltpu.VMEM((experts, rows_w, hcols), bf),
+            pltpu.VMEM((experts, rows_d, dcols), bf),
+            pltpu.VMEM((per, features, hcols), bf),
+            pltpu.VMEM((per, features, hcols), bf),
+            pltpu.VMEM((per, hidden, dcols), bf),
+            pltpu.VMEM((groups, 3, rows_w, hcols), bf),
+            pltpu.VMEM((groups, tok_count, total), bf),
+            pltpu.VMEM((ranks, groups, per, tok_count, hcols), bf),
+            pltpu.VMEM((ranks, tok_count, hcols), bf),
+            pltpu.VMEM((groups, tok_count, dcols), bf),
+            pltpu.VMEM((groups, tok_count, dcols), bf),
+            pltpu.VMEM((tok_count, dcols), f32),
+            dma((3,)),
+            dma((4,)),
+            dma((3, groups)),
+            dma((3, groups)),
+            dma((4 * nz,)),
+            dma((groups,)),
+            dma((groups,)),
+            dma((groups,)),
+            dma((4 * nz,)),
+            dma((groups,)),
+            dma((groups,)),
+            dma((groups,)),
+            dma((groups,)),
+            dma((4, groups)),
+            dma((ranks,)),
+            dma((ranks,)),
+            dma((groups,)),
+            dma((groups,)),
+            dma((3,)),
+            dma((groups, 4)),
+        ],
+        compiler_params=pltpu.CompilerParams(
+            collective_id=0, has_side_effects=True, vmem_limit_bytes=60 * 1024 * 1024
+        ),
+    )(
+        ext,
+        norm_gain[:, None],
+        expert_gate,
+        expert_up,
+        expert_down,
+        shared_gate,
+        shared_up,
+        shared_down,
+    )
 
 
 def expert_hidden(rows, gate_new, up_new):
@@ -32,6 +609,21 @@
     per_group = experts // groups
     tok_count = tokens.shape[0]
     capacity = 2 * tok_count * TOP_K // experts
+    ranks = lax.axis_size("tp")
+    square = expert_down.shape[1] * expert_down.shape[2] == shared_gate.size
+    if capacity >= tok_count and groups & (groups - 1) == 0 and ranks == 4 and square:
+        return dense_body(
+            tokens,
+            norm_gain,
+            expert_gate,
+            expert_up,
+            expert_down,
+            shared_gate,
+            shared_up,
+            shared_down,
+            expert_ids,
+            route_weights,
+        )
     gate_local = (expert_gate * norm_gain[None, :, None]).astype(jnp.bfloat16)
     up_local = (expert_up * norm_gain[None, :, None]).astype(jnp.bfloat16)
     down_local = expert_down.astype(jnp.bfloat16)

time: 498 us -> 245 us (0.49)
  waiting for transfers between devices: 227 us -> 0 us
  Pallas kernels: 0 us -> 226 us
  blocking collectives: 132 us -> 0 us
  local copies, waits for them, and re-layouts: 47 us -> 14.6 us
  matrix products: 32.2 us -> 0 us
  starting transfers between devices: 19.2 us -> 0 us
  other arithmetic: 21.2 us -> 2.42 us
  between operations: 14 us -> 0.7 us
    pallas_call x0 -> x1, Pallas kernels: none -> 226 us  [dense_body(): pl.pallas_call(functools.partial(fused_kernel, groups, ranks), out_shape=...]
    all_gather x5 -> x0, waiting for transfers between devices: 139 us -> none  [the longest x1 53.6 us: body(): lax.all_gather(shared_second_local, 'fs', axis=0, tiled=True)]
    all_to_all x2 -> x0, blocking collectives: 125 us -> none  [the longest x1 74.1 us: body(): lax.all_to_all(mine, 'fs', split_axis=0, concat_axis=0, tiled=True)]
    all_to_all x3 -> x0, waiting for transfers between devices: 87.4 us -> none  [the longest x1 45.2 us: body(): lax.all_to_all(down_local, 'fs', split_axis=0, concat_axis=2, tiled=True)]
    dot_general x6 -> x0, matrix products: 32.2 us -> none  [the longest x1 10.5 us: expert_hidden(): jnp.einsum('secn,enf->secf', rows, gate_new, preferred_element_type=jnp.f...]
    gather x2 -> x0, local copies, waits for them, and re-layouts: 23.1 us -> none  [the longest x1 15.9 us: body(): normed[slot_token.reshape(-1)]]
    all_to_all x3 -> x0, starting transfers between devices: 18.9 us -> none  [the longest x1 6.75 us: body(): lax.all_to_all(routed_total.astype(jnp.bfloat16), 'fs', split_axis=0, con...]
    convert_element_type x6 -> x2, other arithmetic: 12.4 us -> 0.22 us  [the longest x1 0.2 us: dense_body(): (wide * lax.rsqrt(jnp.mean(wide * wide, axis=-1, keepdims=True) + EPS)).a...]
  transfers between devices with their start and end apart: 8 -> 0, of which waited for: 5 -> 0; matrix products, arithmetic and copies ran while one was open for 6% -> 0% of each run, Pallas kernels for 0% -> 0%
where the time goes in v1:
time: 245 us; the launch traced here: 244 us
  Pallas kernels  226 us (92%)
  local copies, waits for them, and re-layouts  14.6 us (6%)
    pallas_call x1, Pallas kernels, dense_body(): pl.pallas_call(functools.partial(fused_kernel, groups, ranks), out_shape=...  226 us
    unnamed x21, local copies, waits for them, and re-layouts  11.7 us

profile of v1, /device:TPU:30, one launch (start us, length us, event | category | flops | bytes accessed | tf_op | source)
XLA Modules:
  0.0 244.2 jit_solution(15822538745257259562)
XLA Ops:
  0.6 0.0 copy-start
  0.6 1.4 fusion
  2.1 0.7 select_reduce_fusion
  2.9 0.1 copy.27
  3.0 0.1 copy.26
  3.1 0.1 copy.25
  3.2 1.5 copy.28.gain
  4.7 0.0 copy-done
  4.7 0.2 fusion.1
  4.9 1.1 concatenate.3.ext
  6.0 226.4 %shard_map.153 = (bf16[2,2048,256]{2,1,0:T(8,128)(2,1)}, bf16[2,2048,256]{2,1,0:T(8,128)(2,1)}, bf16[2,1024,512]{2,1,0:T(8,128)(2,1)}, bf16[2048,256]{1,0:T(8,12...) custom-call(bf16[192,2176]{1,0:T(8,128)(2,1)} %concatenate.3.ext, ...), custom_call_target="tpu_custom_call" | custom-call | tf_op jit(solution)/shard_map/pallas_call | solution.py:523
  232.4 0.0 copy-start.2
  232.4 3.2 %copy.36 = bf16[2,2048,256]{2,1,0:T(8,128)(2,1)} copy(bf16[2,2048,256]{2,1,0:T(8,128)(2,1)} %get-tuple-element.18) | data formatting | bytes 4194304
  235.6 0.0 copy-done.2
  235.6 0.0 copy-start.1
  235.6 1.3 copy.37
  237.0 1.0 copy-done.1
  238.0 0.0 copy-start.5
  238.0 1.3 copy.38
  239.3 0.6 copy-done.5
  239.9 0.0 copy-start.4
  239.9 0.0 copy-start.3
  239.9 1.0 copy.39
  240.9 0.6 copy-done.4
  241.5 0.0 copy-start.6
  241.5 1.0 copy.40
  242.5 0.0 copy-done.3
  242.5 1.0 copy.41
  243.5 0.0 copy-done.6
  243.5 0.7 copy.42
  (4 shorter events, 0.0 us)
Async XLA Ops:
  0.6 4.0 %copy-start = (bf16[192,2048]{1,0:T(8,128)(2,1)S(1)}, bf16[192,2048]{1,0:T(8,128)(2,1)}, u32[]{:S(2)}) copy-start(bf16[192,2048]{1,0:T(8,128)(2,1)} %param.10) | copy-start | bytes 2359300
  232.4 3.2 %copy-start.2 = (bf16[2,2048,256]{2,1,0:T(8,128)(2,1)S(1)}, bf16[2,2048,256]{2,1,0:T(8,128)(2,1)}, u32[]{:S(2)}) copy-start(bf16[2,2048,256]{2,1,0:T(8,128)(2,1)} %get-tuple-element.19) | copy-start | bytes 6291460
  235.6 2.3 copy-start.1
  238.0 2.0 copy-start.5
  239.9 1.6 copy-start.4
  239.9 2.6 %copy-start.3 = (bf16[1024,512]{1,0:T(8,128)(2,1)S(1)}, bf16[1024,512]{1,0:T(8,128)(2,1)}, u32[]{:S(2)}) copy-start(bf16[1024,512]{1,0:T(8,128)(2,1)} %get-tuple-element.23) | copy-start | bytes 3145732
  241.5 1.9 copy-start.6

commit v2 on v1

--- a/solution.py
+++ b/solution.py
@@ -13,6 +13,7 @@
 
 MESH = pl.DeviceIdType.MESH
 LANES = 128
+VMEM_BYTES = 48 * 1024 * 1024
 
 
 def flip(value, mask, extent):
@@ -35,9 +36,9 @@
     sg,
     su,
     sd,
-    out_g,
-    out_u,
-    out_d,
+    rv_g,
+    rv_u,
+    rv_d,
     out_sg,
     out_su,
     out_sd,
@@ -48,18 +49,18 @@
     sb_g,
     sb_u,
     sb_d,
-    rv_g,
-    rv_u,
-    rv_d,
     sh,
     tok,
     hid,
     shid,
-    res_s,
-    res_r,
+    xs,
+    xr,
+    zs,
+    zr,
     own_out,
     load_sem,
     loc_sem,
+    own_sem,
     a2a_send,
     a2a_recv,
     tok_send,
@@ -74,9 +75,10 @@
     hid_recv,
     shid_send,
     shid_recv,
-    res_send,
-    res_recv,
-    out_sem,
+    x_send,
+    x_recv,
+    z_send,
+    z_recv,
     shout_sem,
 ):
     nx = 2
@@ -104,7 +106,7 @@
     ]
     for load in loads:
         load.start()
-    own_tok = pltpu.make_async_copy(ext, tok.at[me], loc_sem.at[3])
+    own_tok = pltpu.make_async_copy(ext, tok.at[me], loc_sem)
     own_tok.start()
 
     barrier = pltpu.get_barrier_semaphore()
@@ -229,60 +231,63 @@
     order = [o for o in (6, 4, 2, 7, 5, 3, 1) if o < groups]
     order = order + [o for o in range(1, groups) if o not in order]
 
-    def a2a_copy(index, o):
-        sendbuf, recvbuf, rows = (
-            (sb_g, rv_g, rows_w),
-            (sb_u, rv_u, rows_w),
-            (sb_d, rv_d, rows_d),
-        )[index]
+    def a2a_ends(index, piece, owner_at, row_at):
+        if index < 2:
+            sendbuf, recvbuf = ((sb_g, rv_g), (sb_u, rv_u))[index]
+            return (
+                sendbuf.at[owner_at * per + piece],
+                recvbuf.at[piece, pl.ds(row_at * rows_w, rows_w), :],
+            )
+        columns = pl.ds(piece * hw, hw)
+        return (
+            sb_d.at[pl.ds(owner_at * per, per), :, columns],
+            rv_d.at[:, pl.ds(row_at * rows_d, rows_d), columns],
+        )
+
+    def pieces(index):
+        return per if index < 2 else 2
+
+    def a2a_copy(index, piece, o):
         target = flip(me, o, groups)
+        src, dst = a2a_ends(index, piece, target, me)
         return fs_copy(
-            sendbuf.at[pl.ds(target * per, per)],
-            recvbuf.at[:, pl.ds(me * rows, rows), :],
-            a2a_send.at[index, o],
-            a2a_recv.at[index, o],
-            target,
-        )
-
-    def a2a_own(index):
-        sendbuf, recvbuf, rows = (
-            (sb_g, rv_g, rows_w),
-            (sb_u, rv_u, rows_w),
-            (sb_d, rv_d, rows_d),
-        )[index]
-        return pltpu.make_async_copy(
-            sendbuf.at[pl.ds(me * per, per)],
-            recvbuf.at[:, pl.ds(me * rows, rows), :],
-            loc_sem.at[index],
-        )
-
-    def a2a_start(index):
+            src, dst, a2a_send.at[index, piece, o], a2a_recv.at[index, piece, o], target
+        )
+
+    def a2a_own(index, piece):
+        src, dst = a2a_ends(index, piece, me, me)
+        return pltpu.make_async_copy(src, dst, own_sem.at[index, piece])
+
+    def a2a_start(index, piece):
         for o in order:
-            a2a_copy(index, o).start()
-        a2a_own(index).start()
-
-    def a2a_arrive(index, recvbuf, out):
+            a2a_copy(index, piece, o).start()
+        a2a_own(index, piece).start()
+
+    def a2a_arrive(index, piece):
         for o in order:
-            a2a_copy(index, o).wait_recv()
-        a2a_own(index).wait()
-        pltpu.make_async_copy(recvbuf, out, out_sem.at[index]).start()
+            a2a_copy(index, piece, o).wait_recv()
+        a2a_own(index, piece).wait()
 
     loads[0].wait()
     cast(st_g, sb_g, True)
     gather_moves(sh_copy, nothing, 0, start)
     gather_moves(tok_copy, tok_arrive, 1, start)
-    a2a_start(0)
+    a2a_start(0, 0)
     loads[1].wait()
     cast(st_u, sb_u, True)
     gather_moves(sh_copy, sh_arrive, 1, start)
     for step in range(2, nz):
         gather_moves(tok_copy, tok_arrive, step, start)
         if step == 2:
-            a2a_start(1)
+            a2a_start(1, 0)
+            for piece in range(1, per):
+                a2a_start(0, piece)
+                a2a_start(1, piece)
             loads[2].wait()
             cast(st_d, sb_d, False)
         gather_moves(sh_copy, sh_arrive, step, start)
-    a2a_start(2)
+    a2a_start(2, 0)
+    a2a_start(2, 1)
 
     for zz in range(nz):
         tok_arrive(zz * nx + (1 - x))
@@ -339,80 +344,94 @@
     for o in range(1, ranks):
         shid_copy(o).start()
 
-    a2a_arrive(0, rv_g, out_g)
-    a2a_arrive(1, rv_u, out_u)
-
-    def hid_core(block):
+    def hid_core(e, block):
         return tp_copy(
-            hid.at[tp, block], hid.at[tp, block], hid_csend.at[block], hid_recv.at[1, block], partner
-        )
-
-    def hid_across(block):
+            hid.at[tp, block, e],
+            hid.at[tp, block, e],
+            hid_csend.at[e, block],
+            hid_recv.at[0, e, block],
+            partner,
+        )
+
+    def hid_across(e, block):
         return tp_copy(
-            hid.at[tp, block], hid.at[tp, block], hid_ysend.at[block], hid_recv.at[2, block], across
-        )
-
-    def hid_forward(block):
+            hid.at[tp, block, e],
+            hid.at[tp, block, e],
+            hid_ysend.at[e, block],
+            hid_recv.at[1, e, block],
+            across,
+        )
+
+    def hid_forward(e, block):
         return tp_copy(
-            hid.at[across, block],
-            hid.at[across, block],
-            hid_fsend.at[block],
-            hid_recv.at[3, block],
+            hid.at[across, block, e],
+            hid.at[across, block, e],
+            hid_fsend.at[e, block],
+            hid_recv.at[2, e, block],
             partner,
         )
 
     def turn(o):
         return (me + o) % groups
 
-    @pl.loop(0, groups)
-    def _(o):
-        block = turn(o + 1)
-        rows = tok[block, :, 0:features]
-        for e in range(per):
+    def shared_out():
+        for o in range(1, ranks):
+            shid_copy(o).wait_recv()
+        for part in range(2):
+            total = jnp.zeros((tok_count, hw), jnp.float32)
+            for block in range(groups):
+                at = block * rows_d
+                total = total + jnp.dot(
+                    shid[at // hcols, :, at % hcols : at % hcols + rows_d],
+                    sh[block, 2, part * rows_d : (part + 1) * rows_d],
+                    preferred_element_type=jnp.float32,
+                )
+            own_out[:, part * hw : (part + 1) * hw] = total
+
+    for e in range(per):
+        a2a_arrive(0, e)
+        a2a_arrive(1, e)
+
+        @pl.loop(0, groups)
+        def _(o):
+            block = turn(o + 1)
+            rows = tok[block, :, 0:features]
             first = jnp.dot(rows, rv_g[e], preferred_element_type=jnp.float32)
             second = jnp.dot(rows, rv_u[e], preferred_element_type=jnp.float32)
             hid[tp, block, e] = (jax.nn.silu(first) * second).astype(jnp.bfloat16)
 
-        @pl.when(o >= 1)
-        def _():
-            before = turn(o)
-            hid_across(before).start()
-            hid_core(before).start()
-
-    for o in range(1, ranks):
-        shid_copy(o).wait_recv()
-    hid_across(me).start()
-    hid_core(me).start()
-    for part in range(2):
+            @pl.when(o >= 1)
+            def _():
+                before = turn(o)
+                hid_across(e, before).start()
+                hid_core(e, before).start()
+
+        if e == 0:
+            shared_out()
+        else:
+            hid_across(e - 1, turn(1)).wait_recv()
+            hid_forward(e - 1, turn(1)).start()
+        hid_across(e, me).start()
+        hid_core(e, me).start()
+
+        @pl.loop(0 if e == per - 1 else 1, groups)
+        def _(o):
+            block = turn(o + 1)
+            hid_across(e, block).wait_recv()
+            hid_forward(e, block).start()
+
+    @pl.loop(1, groups + 1)
+    def _(o):
+        block = turn(o)
+        for e in range(per):
+            hid_core(e, block).wait_recv()
+            hid_forward(e, block).wait_recv()
+
+    lanes = lax.broadcasted_iota(jnp.int32, (tok_count, LANES), 1)
+
+    def block_out(block, half_at):
+        table = tok[block, :, features : features + LANES].astype(jnp.float32)
         total = jnp.zeros((tok_count, hw), jnp.float32)
-        for block in range(groups):
-            at = block * rows_d
-            total = total + jnp.dot(
-                shid[at // hcols, :, at % hcols : at % hcols + rows_d],
-                sh[block, 2, part * rows_d : (part + 1) * rows_d],
-                preferred_element_type=jnp.float32,
-            )
-        own_out[:, part * hw : (part + 1) * hw] = total
-
-    @pl.loop(0, groups)
-    def _(o):
-        block = turn(o + 1)
-        hid_across(block).wait_recv()
-        hid_forward(block).start()
-
-    a2a_arrive(2, rv_d, out_d)
-
-    lanes = lax.broadcasted_iota(jnp.int32, (tok_count, LANES), 1)
-
-    def res_copy(o):
-        target = turn(o)
-        return fs_copy(
-            res_s.at[target], res_r.at[me], res_send.at[o], res_recv.at[o], target
-        )
-
-    def block_out(block):
-        table = tok[block, :, features : features + LANES].astype(jnp.float32)
-        total = jnp.zeros((tok_count, dcols), jnp.float32)
         for e in range(per):
             expert = me * per + e
             weight = jnp.sum(
@@ -424,44 +443,88 @@
                 axis=1,
                 keepdims=True,
             )
-            out = jnp.zeros((tok_count, dcols), jnp.float32)
+            out = jnp.zeros((tok_count, hw), jnp.float32)
             for r in range(ranks):
                 out = out + jnp.dot(
                     hid[r, block, e],
-                    rv_d[e, r * hcols : (r + 1) * hcols],
+                    rv_d[e, r * hcols : (r + 1) * hcols, half_at * hw : (half_at + 1) * hw],
                     preferred_element_type=jnp.float32,
                 )
             total = total + weight * out
         return total
 
-    @pl.loop(1, groups + 1)
-    def _(o):
-        block = turn(o)
-        hid_core(block).wait_recv()
-        hid_forward(block).wait_recv()
-
-        @pl.when(o < groups)
-        def _():
-            res_s[block] = block_out(block).astype(jnp.bfloat16)
-
-        @pl.when(o == groups)
-        def _():
-            own_out[...] = own_out[...] + block_out(block)
-
-        @pl.when(o >= 2)
-        def _():
-            res_copy(o - 1).start()
-
-    for o in range(1, groups):
-        res_copy(o).wait_recv()
-        own_out[...] = own_out[...] + res_r[(me + groups - o) % groups].astype(jnp.float32)
-    out_mixed[...] = own_out[...].astype(jnp.bfloat16)
-
-    for o in range(1, groups):
-        res_copy(o).wait_send()
+    def x_copy(part, zz):
+        return fs_copy(
+            xs.at[part, zz],
+            xr.at[part, zz],
+            x_send.at[part, zz],
+            x_recv.at[part, zz],
+            z * nx + (1 - x),
+        )
+
+    def z_copy(part, j):
+        zz = (z + j) % nz
+        return fs_copy(
+            zs.at[part, zz], zr.at[part, z], z_send.at[part, j], z_recv.at[part, j], zz * nx + x
+        )
+
+    def x_stage(part):
+        @pl.loop(1, nz + 1)
+        def _(j):
+            zz = (z + j) % nz
+            xs[part, zz] = block_out(zz * nx + (1 - x), part).astype(jnp.bfloat16)
+
+            @pl.when(j >= 2)
+            def _():
+                x_copy(part, (z + j - 1) % nz).start()
+
+    def z_stage(part):
+        @pl.loop(1, nz + 1)
+        def _(j):
+            zz = (z + j) % nz
+            total = block_out(zz * nx + x, part)
+
+            @pl.when(j == 1)
+            def _():
+                x_copy(part, z).start()
+
+            x_copy(part, zz).wait_recv()
+            total = total + xr[part, zz].astype(jnp.float32)
+
+            @pl.when(j < nz)
+            def _():
+                zs[part, zz] = total.astype(jnp.bfloat16)
+
+            @pl.when(j == nz)
+            def _():
+                columns = slice(part * hw, (part + 1) * hw)
+                own_out[:, columns] = own_out[:, columns] + total
+
+            @pl.when(j >= 2)
+            def _():
+                z_copy(part, j - 1).start()
+
+    for part in range(2):
+        a2a_arrive(2, part)
+        x_stage(part)
+        z_stage(part)
+
+    for part in range(2):
+        columns = slice(part * hw, (part + 1) * hw)
+        for j in range(1, nz):
+            z_copy(part, j).wait_recv()
+            own_out[:, columns] = own_out[:, columns] + zr[part, (z + nz - j) % nz].astype(jnp.float32)
+        out_mixed[:, columns] = own_out[:, columns].astype(jnp.bfloat16)
+
+    for part in range(2):
+        for j in range(nz):
+            x_copy(part, j).wait_send()
+        for j in range(1, nz):
+            z_copy(part, j).wait_send()
     for index in range(3):
-        for o in order:
-            a2a_copy(index, o).wait_send()
+        for piece in range(pieces(index)):
+            for o in order:
+                a2a_copy(index, piece, o).wait_send()
     for step in range(nz):
         gather_moves(tok_copy, nothing, step, wait_send)
         gather_moves(sh_copy, nothing, step, wait_send)
@@ -472,12 +535,11 @@
 
     @pl.loop(0, groups)
     def _(o):
-        hid_core(o).wait_send()
-        hid_across(o).wait_send()
-        hid_forward(o).wait_send()
-
-    for index, (recvbuf, out) in enumerate(((rv_g, out_g), (rv_u, out_u), (rv_d, out_d))):
-        pltpu.make_async_copy(recvbuf, out, out_sem.at[index]).wait()
+        for e in range(per):
+            hid_core(e, o).wait_send()
+            hid_across(e, o).wait_send()
+            hid_forward(e, o).wait_send()
+
     for block in range(groups):
         for part in range(4):
             sh_out(block, part).wait()
@@ -523,16 +585,16 @@
     return pl.pallas_call(
         functools.partial(fused_kernel, groups, ranks),
         out_shape=(
-            jax.ShapeDtypeStruct((per, features, hcols), bf),
-            jax.ShapeDtypeStruct((per, features, hcols), bf),
-            jax.ShapeDtypeStruct((per, hidden, dcols), bf),
-            jax.ShapeDtypeStruct((features, hcols), bf),
-            jax.ShapeDtypeStruct((features, hcols), bf),
-            jax.ShapeDtypeStruct((hidden, dcols), bf),
-            jax.ShapeDtypeStruct((tok_count, dcols), bf),
+            pltpu.VMEM((per, features, hcols), bf),
+            pltpu.VMEM((per, features, hcols), bf),
+            pltpu.VMEM((per, hidden, dcols), bf),
+            pltpu.VMEM((features, hcols), bf),
+            pltpu.VMEM((features, hcols), bf),
+            pltpu.VMEM((hidden, dcols), bf),
+            pltpu.VMEM((tok_count, dcols), bf),
         ),
         in_specs=[vmem, vmem, any_space, any_space, any_space, vmem, vmem, vmem],
-        out_specs=(any_space,) * 6 + (vmem,),
+        out_specs=(vmem,) * 7,
         scratch_shapes=[
             pltpu.VMEM((experts, rows_w, hcols), f32),
             pltpu.VMEM((experts, rows_w, hcols), f32),
@@ -540,39 +602,40 @@
             pltpu.VMEM((experts, rows_w, hcols), bf),
             pltpu.VMEM((experts, rows_w, hcols), bf),
             pltpu.VMEM((experts, rows_d, dcols), bf),
-            pltpu.VMEM((per, features, hcols), bf),
-            pltpu.VMEM((per, features, hcols), bf),
-            pltpu.VMEM((per, hidden, dcols), bf),
             pltpu.VMEM((groups, 3, rows_w, hcols), bf),
             pltpu.VMEM((groups, tok_count, total), bf),
             pltpu.VMEM((ranks, groups, per, tok_count, hcols), bf),
             pltpu.VMEM((ranks, tok_count, hcols), bf),
-            pltpu.VMEM((groups, tok_count, dcols), bf),
-            pltpu.VMEM((groups, tok_count, dcols), bf),
+            pltpu.VMEM((2, nz, tok_count, dcols // 2), bf),
+            pltpu.VMEM((2, nz, tok_count, dcols // 2), bf),
+            pltpu.VMEM((2, nz, tok_count, dcols // 2), bf),
+            pltpu.VMEM((2, nz, tok_count, dcols // 2), bf),
             pltpu.VMEM((tok_count, dcols), f32),
             dma((3,)),
-            dma((4,)),
-            dma((3, groups)),
-            dma((3, groups)),
+            dma,
+            dma((3, max(per, 2))),
+            dma((3, max(per, 2), groups)),
+            dma((3, max(per, 2), groups)),
             dma((4 * nz,)),
             dma((groups,)),
             dma((groups,)),
             dma((groups,)),
             dma((4 * nz,)),
             dma((groups,)),
-            dma((groups,)),
-            dma((groups,)),
-            dma((groups,)),
-            dma((4, groups)),
+            dma((per, groups)),
+            dma((per, groups)),
+            dma((per, groups)),
+            dma((3, per, groups)),
             dma((ranks,)),
             dma((ranks,)),
-            dma((groups,)),
-            dma((groups,)),
-            dma((3,)),
+            dma((2, nz)),
+            dma((2, nz)),
+            dma((2, nz)),
+            dma((2, nz)),
             dma((groups, 4)),
         ],
         compiler_params=pltpu.CompilerParams(
-            collective_id=0, has_side_effects=True, vmem_limit_bytes=60 * 1024 * 1024
+            collective_id=0, has_side_effects=True, vmem_limit_bytes=VMEM_BYTES
         ),
     )(
         ext,

time: 245 us -> 220 us (0.90); the launches traced: 244 us -> 216 us
  Pallas kernels: 226 us -> 203 us
  local copies, waits for them, and re-layouts: 14.6 us -> 10.4 us
    pallas_call x1, Pallas kernels: 226 us -> 203 us  [dense_body(): pl.pallas_call(functools.partial(fused_kernel, groups, ranks), out_shape=...]
    unnamed x21 -> x9, local copies, waits for them, and re-layouts: 11.7 us -> 7.55 us
where the time goes in v2:
time: 220 us; the launch traced here: 216 us
  Pallas kernels  203 us (92%)
  local copies, waits for them, and re-layouts  10.4 us (5%)
  other arithmetic  2.42 us (1%)
    pallas_call x1, Pallas kernels, dense_body(): pl.pallas_call(functools.partial(fused_kernel, groups, ranks), out_shape=...  203 us
    unnamed x9, local copies, waits for them, and re-layouts  7.55 us

profile of v2, /device:TPU:30, one launch (start us, length us, event | category | flops | bytes accessed | tf_op | source)
XLA Modules:
  0.0 216.4 jit_solution(9377758405696256561)
XLA Ops:
  0.6 0.0 copy-start
  0.6 1.4 fusion
  2.1 0.7 select_reduce_fusion
  2.9 0.1 copy.27
  3.0 0.1 copy.26
  3.1 0.1 copy.25
  3.2 1.5 copy.28.gain
  4.7 0.0 copy-done
  4.7 0.2 fusion.1
  4.9 1.1 concatenate.3.ext
  6.0 202.9 %shard_map.153 = (bf16[2,2048,256]{2,1,0:T(8,128)(2,1)S(1)}, bf16[2,2048,256]{2,1,0:T(8,128)(2,1)S(1)}, bf16[2,1024,512]{2,1,0:T(8,128)(2,1)S(1)}, bf16[2048,256...) custom-call(bf16[192,2176]{1,0:T(8,128)(2,1)} %concatenate.3.ext, ...), custom_call_target="tpu_custom_call" | custom-call | tf_op jit(solution)/shard_map/pallas_call | solution.py:585
  208.9 1.3 copy.36
  210.2 0.7 copy.42
  210.9 1.0 copy.39
  211.8 1.0 copy.40
  212.8 1.0 copy.41
  213.8 1.3 copy.37
  215.1 1.3 copy.38
  (4 shorter events, 0.0 us)
Async XLA Ops:
  0.6 4.0 %copy-start = (bf16[192,2048]{1,0:T(8,128)(2,1)S(1)}, bf16[192,2048]{1,0:T(8,128)(2,1)}, u32[]{:S(2)}) copy-start(bf16[192,2048]{1,0:T(8,128)(2,1)} %param.10) | copy-start | bytes 2359300

commit v3 on v2

--- a/solution.py
+++ b/solution.py
@@ -65,8 +65,8 @@
     a2a_recv,
     tok_send,
     tok_recv,
-    tok_csend,
-    tok_crecv,
+    tok_tsend,
+    tok_trecv,
     sh_send,
     sh_recv,
     hid_csend,
@@ -86,7 +86,6 @@
     me = lax.axis_index("fs")
     tp = lax.axis_index("tp")
     z, x = me // nx, me % nx
-    core = tp % 2
     partner = flip(tp, 1, ranks)
     across = flip(tp, 2, ranks)
     per = eg.shape[0] // groups
@@ -95,7 +94,7 @@
     rows_d = ed.shape[1]
     tok_count = ext.shape[0]
     width = st_d.shape[2] * ranks
-    half = tok_count // 2
+    share = tok_count // ranks
     hcols = eg.shape[2]
     dcols = ed.shape[2]
     hw = dcols // 2
@@ -120,8 +119,8 @@
         )
     pl.semaphore_wait(barrier, groups + ranks - 2)
 
-    mine = pl.ds(core * half, half)
-    theirs = pl.ds((1 - core) * half, half)
+    mine = pl.ds(tp * share, share)
+    theirs = pl.ds(across * share, share)
 
     def fs_copy(src, dst, send, recv, target):
         return pltpu.make_async_remote_copy(
@@ -198,15 +197,17 @@
 
     def tok_arrive(block):
         tok_copy(block, 0, me).wait_recv()
-        core_copy(block).start()
-
-    def core_copy(block):
+        tok_share(0, block).start()
+        tok_share(1, block).start()
+
+    def tok_share(kind, block):
+        rows = theirs if kind == 2 else mine
         return tp_copy(
-            tok.at[block, mine],
-            tok.at[block, mine],
-            tok_csend.at[block],
-            tok_crecv.at[block],
-            partner,
+            tok.at[block, rows],
+            tok.at[block, rows],
+            tok_tsend.at[kind, block],
+            tok_trecv.at[kind, block],
+            across if kind == 1 else partner,
         )
 
     def sh_arrive(block):
@@ -228,7 +229,7 @@
                 value = value * gain[...]
             sendbuf[e] = value.astype(jnp.bfloat16)
 
-    order = [o for o in (6, 4, 2, 7, 5, 3, 1) if o < groups]
+    order = [o for o in (7, 5, 6, 4, 3, 2, 1) if o < groups]
     order = order + [o for o in range(1, groups) if o not in order]
 
     def a2a_ends(index, piece, owner_at, row_at):
@@ -275,25 +276,25 @@
     a2a_start(0, 0)
     loads[1].wait()
     cast(st_u, sb_u, True)
-    gather_moves(sh_copy, sh_arrive, 1, start)
     for step in range(2, nz):
         gather_moves(tok_copy, tok_arrive, step, start)
         if step == 2:
             a2a_start(1, 0)
-            for piece in range(1, per):
-                a2a_start(0, piece)
-                a2a_start(1, piece)
             loads[2].wait()
             cast(st_d, sb_d, False)
-        gather_moves(sh_copy, sh_arrive, step, start)
-    a2a_start(2, 0)
-    a2a_start(2, 1)
+            gather_moves(sh_copy, sh_arrive, 1, start)
 
     for zz in range(nz):
         tok_arrive(zz * nx + (1 - x))
-    for zz in range(nz):
-        sh_arrive(zz * nx + (1 - x))
     own_tok.wait()
+    for o in range(1, groups):
+        tok_share(1, flip(me, o, groups)).wait_recv()
+        tok_share(2, flip(me, o, groups)).start()
+    for piece in range(1, per):
+        a2a_start(0, piece)
+        a2a_start(1, piece)
+    for step in range(2, nz - 1):
+        gather_moves(sh_copy, sh_arrive, step, start)
 
     def sh_out(block, part):
         src_dst = (
@@ -303,10 +304,6 @@
             (sh.at[block, 2, pl.ds(rows_d, rows_d)], out_sd.at[pl.ds(block * rows_d, rows_d), pl.ds(hw, hw)]),
         )[part]
         return pltpu.make_async_copy(*src_dst, shout_sem.at[block, part])
-
-    for block in range(groups):
-        for part in range(4):
-            sh_out(block, part).start()
 
     features = groups * rows_w
 
@@ -320,29 +317,24 @@
             )
         return total
 
-    shared_first = shared_half(0)
-    shared_second = shared_half(1)
-    shid[tp] = (jax.nn.silu(shared_first) * shared_second).astype(jnp.bfloat16)
+    def shared_hidden():
+        for zz in range(nz):
+            sh_arrive(zz * nx + (1 - x))
+        for block in range(groups):
+            for part in range(4):
+                sh_out(block, part).start()
+        first = shared_half(0)
+        second = shared_half(1)
+        shid[tp] = (jax.nn.silu(first) * second).astype(jnp.bfloat16)
 
     def shid_copy(o):
         return tp_copy(
             shid.at[tp], shid.at[tp], shid_send.at[o], shid_recv.at[o], flip(tp, o, ranks)
         )
 
-    def core_arrive(block):
-        tp_copy(
-            tok.at[block, theirs],
-            tok.at[block, theirs],
-            tok_csend.at[block],
-            tok_crecv.at[block],
-            partner,
-        ).wait_recv()
-
     for o in range(1, groups):
-        core_arrive(flip(me, o, groups))
-
-    for o in range(1, ranks):
-        shid_copy(o).start()
+        tok_share(0, flip(me, o, groups)).wait_recv()
+        tok_share(2, flip(me, o, groups)).wait_recv()
 
     def hid_core(e, block):
         return tp_copy(
@@ -391,6 +383,9 @@
     for e in range(per):
         a2a_arrive(0, e)
         a2a_arrive(1, e)
+        if e == 0:
+            a2a_start(2, 0)
+            a2a_start(2, 1)
 
         @pl.loop(0, groups)
         def _(o):
@@ -406,11 +401,11 @@
                 hid_across(e, before).start()
                 hid_core(e, before).start()
 
-        if e == 0:
-            shared_out()
-        else:
+        if e > 0:
             hid_across(e - 1, turn(1)).wait_recv()
             hid_forward(e - 1, turn(1)).start()
+        if e == per - 1:
+            shared_hidden()
         hid_across(e, me).start()
         hid_core(e, me).start()
 
@@ -419,6 +414,14 @@
             block = turn(o + 1)
             hid_across(e, block).wait_recv()
             hid_forward(e, block).start()
+
+        if e == 0:
+            gather_moves(sh_copy, sh_arrive, nz - 1, start)
+        if e == per - 1:
+            for o in range(1, ranks):
+                shid_copy(o).start()
+
+    shared_out()
 
     @pl.loop(1, groups + 1)
     def _(o):
@@ -529,7 +532,8 @@
         gather_moves(tok_copy, nothing, step, wait_send)
         gather_moves(sh_copy, nothing, step, wait_send)
     for o in range(1, groups):
-        core_copy(flip(me, o, groups)).wait_send()
+        for kind in range(3):
+            tok_share(kind, flip(me, o, groups)).wait_send()
     for o in range(1, ranks):
         shid_copy(o).wait_send()
 
@@ -618,8 +622,8 @@
             dma((3, max(per, 2), groups)),
             dma((4 * nz,)),
             dma((groups,)),
-            dma((groups,)),
-            dma((groups,)),
+            dma((3, groups)),
+            dma((3, groups)),
             dma((4 * nz,)),
             dma((groups,)),
             dma((per, groups)),
@@ -674,7 +678,7 @@
     capacity = 2 * tok_count * TOP_K // experts
     ranks = lax.axis_size("tp")
     square = expert_down.shape[1] * expert_down.shape[2] == shared_gate.size
-    if capacity >= tok_count and groups & (groups - 1) == 0 and ranks == 4 and square:
+    if capacity >= tok_count and per_group >= 2 and groups >= 8 and groups & (groups - 1) == 0 and ranks == 4 and square:
         return dense_body(
             tokens,
             norm_gain,

time: 220 us -> 215 us (0.977)
  Pallas kernels: 203 us -> 198 us
    pallas_call x1, Pallas kernels: 203 us -> 198 us  [dense_body(): pl.pallas_call(functools.partial(fused_kernel, groups, ranks), out_shape=...]
where the time goes in v3:
time: 215 us; the launch traced here: 212 us
  Pallas kernels  198 us (92%)
  local copies, waits for them, and re-layouts  10.4 us (5%)
  other arithmetic  2.42 us (1%)
    pallas_call x1, Pallas kernels, dense_body(): pl.pallas_call(functools.partial(fused_kernel, groups, ranks), out_shape=...  198 us
    unnamed x9, local copies, waits for them, and re-layouts  7.55 us

profile of v3, /device:TPU:30, one launch (start us, length us, event | category | flops | bytes accessed | tf_op | source)
XLA Modules:
  0.0 211.5 jit_solution(5555134775741975520)
XLA Ops:
  0.6 0.0 copy-start
  0.6 1.4 fusion
  2.1 0.7 select_reduce_fusion
  2.9 0.1 copy.27
  3.0 0.1 copy.26
  3.1 0.1 copy.25
  3.2 1.5 copy.28.gain
  4.7 0.0 copy-done
  4.7 0.2 fusion.1
  4.9 1.1 concatenate.3.ext
  6.0 198.0 %shard_map.153 = (bf16[2,2048,256]{2,1,0:T(8,128)(2,1)S(1)}, bf16[2,2048,256]{2,1,0:T(8,128)(2,1)S(1)}, bf16[2,1024,512]{2,1,0:T(8,128)(2,1)S(1)}, bf16[2048,256...) custom-call(bf16[192,2176]{1,0:T(8,128)(2,1)} %concatenate.3.ext, ...), custom_call_target="tpu_custom_call" | custom-call | tf_op jit(solution)/shard_map/pallas_call | solution.py:589
  204.0 1.3 copy.36
  205.3 0.7 copy.42
  206.0 1.0 copy.39
  206.9 1.0 copy.40
  207.9 1.0 copy.41
  208.9 1.3 copy.37
  210.2 1.3 copy.38
  (4 shorter events, 0.0 us)
Async XLA Ops:
  0.6 4.0 %copy-start = (bf16[192,2048]{1,0:T(8,128)(2,1)S(1)}, bf16[192,2048]{1,0:T(8,128)(2,1)}, u32[]{:S(2)}) copy-start(bf16[192,2048]{1,0:T(8,128)(2,1)} %param.10) | copy-start | bytes 2359300
